TPU v7x, 32 devices: a whole 2x2x4 slice. The times are simulated.
32 devices in a mesh: fs: 8 (over z, x), tp: 4 (over y, core).
Axes of the slice: x: 2, y: 2, z: 4, core: 2. Of those that a mesh axis runs over, the one named last changes fastest.
Arguments:
- tokens: bfloat16 [8192, 2048], P('fs', 'tp'), may hold values from -50 to 50
- norm_gain: float32 [2048], P('fs'), may hold values from 0.1 to 1.9
- gate_weight: float32 [2048, 2816], P('fs', 'tp'), may hold values from -0.125 to 0.125
- up_weight: float32 [2048, 2816], P('fs', 'tp'), may hold values from -0.125 to 0.125
- down_weight: float32 [2816, 2048], P('fs', 'tp'), may hold values from -0.109375 to 0.109375
Outputs:
- gate_sampler: bfloat16 [2048, 2816], P(None, 'tp')
- up_sampler: bfloat16 [2048, 2816], P(None, 'tp')
- down_sampler: bfloat16 [2816, 2048], P('tp')
- mixed: bfloat16 [8192, 2048], P('fs', 'tp')
All inputs are finite; a program needn't handle non-finite values.
Results may differ from a plain program's by a relative error of at most 0.0095.
Values may be sent and summed in bfloat16 or wider, within the bound.
A program may use at most 128 MiB of HBM per device.

v0:
```python
import jax
import jax.numpy as jnp
from jax import lax
from jax.sharding import PartitionSpec as P

norm_eps = 1e-06


def shards(tokens, norm_gain, gate_weight, up_weight, down_weight):
    gate_local = (norm_gain[:, None] * gate_weight).astype(jnp.bfloat16)
    up_local = (norm_gain[:, None] * up_weight).astype(jnp.bfloat16)
    down_local = down_weight.astype(jnp.bfloat16)
    gathered = lax.all_gather(tokens, "tp", axis=1, tiled=True)
    floated = gathered.astype(jnp.float32)
    normed = (
        floated * lax.rsqrt(jnp.mean(floated * floated, axis=-1, keepdims=True) + norm_eps)
    ).astype(jnp.bfloat16)
    gate_sampler, up_sampler = (
        lax.all_gather(gate_local, "fs", axis=0, tiled=True),
        lax.all_gather(up_local, "fs", axis=0, tiled=True),
    )
    gate = jnp.dot(normed, gate_sampler, preferred_element_type=jnp.float32)
    up = jnp.dot(normed, up_sampler, preferred_element_type=jnp.float32)
    hidden = (jax.nn.silu(gate) * up).astype(jnp.bfloat16)
    down_columns = lax.all_gather(down_local, "fs", axis=0, tiled=True)
    down_sampler = lax.all_to_all(down_columns, "tp", split_axis=0, concat_axis=1, tiled=True)
    partial_value = jnp.dot(
        lax.all_gather(hidden, "tp", axis=1, tiled=True),
        down_columns,
        preferred_element_type=jnp.float32,
    ).astype(jnp.bfloat16)
    partial_value = lax.optimization_barrier(partial_value)
    summed = partial_value.astype(jnp.float32)
    return (gate_sampler, up_sampler, down_sampler, summed.astype(jnp.bfloat16))


def solution(mesh):
    return jax.shard_map(
        shards,
        mesh=mesh,
        in_specs=(P("fs", "tp"), P("fs"), P("fs", "tp"), P("fs", "tp"), P("fs", "tp")),
        out_specs=(P(None, "tp"), P(None, "tp"), P("tp", None), P("fs", "tp")),
        check_vma=False,
    )
```

profile of v0, /device:TPU:0, one launch (start us, length us, event | category | flops | bytes accessed | tf_op | source)
XLA Modules:
  0.0 316.4 jit_solution(10165208772231586884)
XLA Ops:
  7.2 0.0 copy-start.2
  7.2 0.0 all-gather.12.cloned.1.call-start
  7.2 0.7 all-gather.12.cloned.1.call-update
  7.9 0.0 all-gather.6.cloned.1.call-start
  8.0 2.3 multiply_convert_fusion.1
  10.3 0.0 all-gather.6.cloned.1.call-update
  10.3 0.0 all-gather.8.cloned.1.call-start
  10.3 0.7 all-gather.8.cloned.1.call-update
  11.0 0.0 all-gather.10.cloned.1.call-start
  11.1 0.0 copy-done.2
  11.1 0.8 convert_element_type.25
  11.9 0.0 all-gather.10.cloned.1.call-update
  11.9 0.0 all-gather.14.cloned.1.call-start
  11.9 34.8 %all-gather.12.cloned.1.call-done = bf16[1024,2048]{1,0:T(8,128)(2,1)} async-done(((bf16[1024,512]{1,0:T(8,128)(2,1)}), bf16[1024,2048]{1,0:T(8,128)(2,1)}) %all-gather.12.cloned.1.call-update) | async-done | bytes 4194320 | tf_op jit(solution)/shard_map/all_gather | solution.py:13
  46.8 3.1 fusion
  49.8 59.1 %all-gather.6.cloned.1.call-done = bf16[2048,704]{0,1:T(8,128)(2,1)} async-done(((bf16[256,704]{0,1:T(8,128)(2,1)}), bf16[2048,704]{0,1:T(8,128)(2,1)}) %all-gather.6.cloned.1.call-update) | async-done | bytes 2883600 | tf_op jit(solution)/shard_map/all_gather | solution.py:19
  109.0 6.3 %fusion.3 = f32[1024,704]{0,1:T(8,128)S(1)} fusion(bf16[2048,704]{0,1:T(8,128)(2,1)} %all-gather.6.cloned.1.call-done, bf16[1024,2048]{1,0:T(8,128)(2,1)} %all-gather.12.cloned.1.call-done, f32[1024]{0:T(1024)S(1)} %add_rsqrt_fusion), kind=kOutput, calls=%fused_computation.5 | convolution fusion | flops 2959081472 | bytes 9965568 | tf_op jit(solution)/shard_map/dot_general | solution.py:22
  115.2 54.1 %all-gather.8.cloned.1.call-done = bf16[2048,704]{0,1:T(8,128)(2,1)} async-done(((bf16[256,704]{0,1:T(8,128)(2,1)}), bf16[2048,704]{0,1:T(8,128)(2,1)}) %all-gather.8.cloned.1.call-update) | async-done | bytes 2883600 | tf_op jit(solution)/shard_map/all_gather | solution.py:20
  169.4 7.7 %multiply_convert_fusion = bf16[1024,704]{0,1:T(8,128)(2,1)} fusion(f32[1024,704]{0,1:T(8,128)S(1)} %fusion.3, bf16[2048,704]{0,1:T(8,128)(2,1)} %all-gather.8.cloned.1.call-done, bf16[1024,2048]{1,0:T(8,128)(2,1)} %all-gather.12.cloned.1.call-done, f32[1024]{0:T(1024)S(1)} %add_rsqrt_fusion), kind=kOutput, calls=%fused_computation.4 | convolution fusion | flops 2963406848 | bytes 11407360 | tf_op jit(solution)/shard_map/dot_general | solution.py:23
  177.1 0.0 all-gather.14.cloned.1.call-update
  177.1 50.4 %all-gather.10.cloned.1.call-done = bf16[2816,512]{1,0:T(8,128)(2,1)} async-done(((bf16[352,512]{1,0:T(8,128)(2,1)}), bf16[2816,512]{1,0:T(8,128)(2,1)}) %all-gather.10.cloned.1.call-update) | async-done | bytes 2883600 | tf_op jit(solution)/shard_map/all_gather | solution.py:25
  227.5 64.5 %all_to_all.19 = bf16[4,704,512]{2,1,0:T(8,128)(2,1)S(1)} all-to-all(bf16[4,704,512]{2,1,0:T(8,128)(2,1)} %bitcast.9), channel_id=1, replica_groups=mesh['fs'=8,'tp'=4] {'tp'}, dimensions={0} | all-to-all | bytes 5767168 | tf_op jit(solution)/shard_map/all_to_all | solution.py:26
  292.0 2.0 copy.11
  294.1 0.0 copy-start
  294.1 3.8 %all-gather.14.cloned.1.call-done = bf16[1024,2816]{0,1:T(8,128)(2,1)} async-done(((bf16[1024,704]{0,1:T(8,128)(2,1)}), bf16[1024,2816]{0,1:T(8,128)(2,1)}) %all-gather.14.cloned.1.call-update) | async-done | bytes 5767184 | tf_op jit(solution)/shard_map/all_gather | solution.py:28
  297.8 7.7 %convolution_convert_fusion = bf16[1024,512]{1,0:T(8,128)(2,1)} fusion(bf16[1024,2816]{0,1:T(8,128)(2,1)} %all-gather.14.cloned.1.call-done, bf16[2816,512]{1,0:T(8,128)(2,1)} %all-gather.10.cloned.1.call-done), kind=kOutput, calls=%fused_computation.6 | convolution fusion | flops 2953314304 | bytes 9699328 | tf_op jit(solution)/shard_map/dot_general | solution.py:27
  305.5 0.0 copy-done
  305.5 0.0 copy-start.1
  305.5 1.6 copy.14
  307.0 1.3 copy-done.1
  308.3 1.6 copy.15
  (1 shorter events, 0.0 us)
Async XLA Ops:
  7.2 3.9 %copy-start.2 = (f32[352,512]{1,0:T(8,128)S(1)}, f32[352,512]{1,0:T(8,128)}, u32[]{:S(2)}) copy-start(f32[352,512]{1,0:T(8,128)} %param.9) | copy-start | bytes 2162692
  7.2 39.6 %all-gather.12.cloned.1.call-start = ((), (), s32[]{:S(2)}) async-start(), calls=%async_computation.4 | async-start | bytes 5242880 | tf_op jit(solution)/shard_map/all_gather | solution.py:13
  7.9 101.1 %all-gather.6.cloned.1.call-start = ((), (), s32[]{:S(2)}) async-start(), calls=%async_computation.1 | async-start | bytes 3244032 | tf_op jit(solution)/shard_map/all_gather | solution.py:19
  10.3 159.1 %all-gather.8.cloned.1.call-start = ((), (), s32[]{:S(2)}) async-start(), calls=%async_computation.2 | async-start | bytes 3244032 | tf_op jit(solution)/shard_map/all_gather | solution.py:20
  11.0 216.5 %all-gather.10.cloned.1.call-start = ((), (), s32[]{:S(2)}) async-start(), calls=%async_computation.3 | async-start | bytes 3244032 | tf_op jit(solution)/shard_map/all_gather | solution.py:25
  11.9 285.9 %all-gather.14.cloned.1.call-start = ((), (), s32[]{:S(2)}) async-start(), calls=%async_computation.5 | async-start | bytes 7208960 | tf_op jit(solution)/shard_map/all_gather | solution.py:28
  294.1 11.4 %copy-start = (bf16[2048,704]{0,1:T(8,128)(2,1)S(1)}, bf16[2048,704]{0,1:T(8,128)(2,1)}, u32[]{:S(2)}) copy-start(bf16[2048,704]{0,1:T(8,128)(2,1)} %all-gather.6.cloned.1.call-done) | copy-start | bytes 8650756
  305.5 2.9 copy-start.1
Sparse Core Ops, SparseCore 0:
  9.5 37.1 all-gather.11
  49.4 59.5 all-gather.5
  111.6 57.7 all-gather.7
  172.0 55.4 all-gather.9
  229.5 68.2 all-gather.13
where the time goes:
time: 317 us; the launch traced here: 316 us
  waiting for transfers between devices  204 us (64%)
  blocking collectives  64.5 us (20%)
  matrix products  21.7 us (7%)
  between operations  13.8 us (4%)
  local copies, waits for them, and re-layouts  6.45 us (2%)
  other arithmetic  6.17 us (2%)
    all_to_all x1, blocking collectives, shards(): lax.all_to_all(down_columns, 'tp', split_axis=0, concat_axis=1, tiled=True)  64.5 us
    all_gather x1, waiting for transfers between devices, shards(): lax.all_gather(gate_local, 'fs', axis=0, tiled=True)  59.1 us
    all_gather x1, waiting for transfers between devices, shards(): lax.all_gather(up_local, 'fs', axis=0, tiled=True)  54.1 us
    all_gather x1, waiting for transfers between devices, shards(): down_columns = lax.all_gather(down_local, 'fs', axis=0, tiled=True)  50.4 us
    all_gather x1, waiting for transfers between devices, shards(): gathered = lax.all_gather(tokens, 'tp', axis=1, tiled=True)  34.8 us
    dot_general x1, matrix products, shards(): up = jnp.dot(normed, up_sampler, preferred_element_type=jnp.float32)  7.73 us
    dot_general x1, matrix products, shards(): jnp.dot(lax.all_gather(hidden, 'tp', axis=1, tiled=True), down_columns, p...  7.65 us
  transfers between devices with their start and end apart: 5, of which 5 were waited for; matrix products, arithmetic and copies ran while one was open for 7% of the time, Pallas kernels for 0%

commit v1 on v0

--- a/solution.py
+++ b/solution.py
@@ -2,6 +2,7 @@
 import jax.numpy as jnp
 from jax import lax
 from jax.sharding import PartitionSpec as P
+from jax.lax import all_gather
 
 norm_eps = 1e-06
 
@@ -10,7 +11,8 @@
     gate_local = (norm_gain[:, None] * gate_weight).astype(jnp.bfloat16)
     up_local = (norm_gain[:, None] * up_weight).astype(jnp.bfloat16)
     down_local = down_weight.astype(jnp.bfloat16)
-    gathered = lax.all_gather(tokens, "tp", axis=1, tiled=True)
+    e_next = all_gather(tokens, axis_name="tp")
+    gathered = jnp.concatenate(e_next, axis=1)
     floated = gathered.astype(jnp.float32)
     normed = (
         floated * lax.rsqrt(jnp.mean(floated * floated, axis=-1, keepdims=True) + norm_eps)

time: 317 us -> 317 us (level)
  waiting for transfers between devices: 204 us -> 182 us
  other arithmetic: 6.17 us -> 19.5 us
  local copies, waits for them, and re-layouts: 6.45 us -> 15.3 us
    all_gather x1, waiting for transfers between devices: 59.1 us -> 37 us  [shards(): lax.all_gather(gate_local, 'fs', axis=0, tiled=True)]
    convert_element_type x0 -> x2, other arithmetic: none -> 13.3 us  [the longest x1 6.66 us: shards(): normed = (floated * lax.rsqrt(jnp.mean(floated * floated, axis=-1, keepdi...]
    convert_element_type x0 -> x1, local copies, waits for them, and re-layouts: none -> 8.82 us  [shards(): floated = gathered.astype(jnp.float32)]
  transfers between devices with their start and end apart: 5 -> 5, of which waited for: 5 -> 5; matrix products, arithmetic and copies ran while one was open for 7% -> 14% of each run, Pallas kernels for 0% -> 0%
where the time goes in v1:
time: 317 us; the launch traced here: 316 us
  waiting for transfers between devices  182 us (57%)
  blocking collectives  64.5 us (20%)
  matrix products  20.9 us (7%)
  other arithmetic  19.5 us (6%)
  local copies, waits for them, and re-layouts  15.3 us (5%)
  between operations  13.8 us (4%)
    all_to_all x1, blocking collectives, shards(): lax.all_to_all(down_columns, 'tp', split_axis=0, concat_axis=1, tiled=True)  64.5 us
    all_gather x1, waiting for transfers between devices, shards(): lax.all_gather(up_local, 'fs', axis=0, tiled=True)  54.6 us
    all_gather x1, waiting for transfers between devices, shards(): down_columns = lax.all_gather(down_local, 'fs', axis=0, tiled=True)  50.6 us
    all_gather x1, waiting for transfers between devices, shards(): lax.all_gather(gate_local, 'fs', axis=0, tiled=True)  37 us
    all_gather x1, waiting for transfers between devices, shards(): e_next = all_gather(tokens, axis_name='tp')  34.8 us
    convert_element_type x1, local copies, waits for them, and re-layouts, shards(): floated = gathered.astype(jnp.float32)  8.82 us
    dot_general x1, matrix products, shards(): jnp.dot(lax.all_gather(hidden, 'tp', axis=1, tiled=True), down_columns, p...  7.65 us
    dot_general x1, matrix products, shards(): up = jnp.dot(normed, up_sampler, preferred_element_type=jnp.float32)  7.49 us
  transfers between devices with their start and end apart: 5, of which 5 were waited for; matrix products, arithmetic and copies ran while one was open for 14% of the time, Pallas kernels for 0%

profile of v1, /device:TPU:0, one launch (start us, length us, event | category | flops | bytes accessed | tf_op | source)
XLA Modules:
  0.0 316.4 jit_solution(17140836978841612080)
XLA Ops:
  7.2 0.0 copy-start.2
  7.2 0.0 all-gather.15.cloned.1.call-start
  7.2 0.7 all-gather.15.cloned.1.call-update
  7.9 0.0 all-gather.7.cloned.1.call-start
  8.0 2.3 multiply_convert_fusion.1
  10.3 0.0 all-gather.7.cloned.1.call-update
  10.3 0.0 all-gather.9.cloned.1.call-start
  10.3 0.7 all-gather.9.cloned.1.call-update
  11.0 0.0 all-gather.11.cloned.1.call-start
  11.1 0.0 copy-done.2
  11.1 0.8 convert_element_type.35
  11.9 0.0 all-gather.11.cloned.1.call-update
  11.9 0.0 all-gather.13.cloned.1.call-start
  11.9 34.8 %all-gather.15.cloned.1.call-done = bf16[4096,512]{1,0:T(8,128)(2,1)} async-done(((bf16[1024,512]{1,0:T(8,128)(2,1)}), bf16[4096,512]{1,0:T(8,128)(2,1)}) %all-gather.15.cloned.1.call-update) | async-done | bytes 4194320 | tf_op jit(solution)/shard_map/all_gather | solution.py:14
  46.8 6.6 %convert_bitcast_fusion = f32[1024,4,512]{2,0,1:T(8,128)} fusion(bf16[4096,512]{1,0:T(8,128)(2,1)} %all-gather.15.cloned.1.call-done), kind=kLoop, calls=%fused_computation.1 | loop fusion | flops 2097152 | bytes 12582912 | tf_op jit(solution)/shard_map/convert_element_type | solution.py:16
  53.4 8.8 %copy.15 = f32[1024,4,512]{0,2,1:T(8,128)} copy(f32[1024,4,512]{2,0,1:T(8,128)} %convert_bitcast_fusion) | data formatting | bytes 16777216 | tf_op jit(solution)/shard_map/convert_element_type | solution.py:16
  62.2 3.1 fusion
  65.3 6.7 %fusion.1 = bf16[1024,2048]{0,1:T(8,128)(2,1)} fusion(f32[1024,4,512]{0,2,1:T(8,128)} %copy.15, f32[1024]{0:T(1024)S(1)} %add_rsqrt_fusion), kind=kLoop, calls=%fused_computation.4 | loop fusion | flops 4194304 | bytes 12587008 | tf_op jit(solution)/shard_map/convert_element_type | solution.py:19
  71.9 37.0 %all-gather.7.cloned.1.call-done = bf16[2048,704]{0,1:T(8,128)(2,1)} async-done(((bf16[256,704]{0,1:T(8,128)(2,1)}), bf16[2048,704]{0,1:T(8,128)(2,1)}) %all-gather.7.cloned.1.call-update) | async-done | bytes 2883600 | tf_op jit(solution)/shard_map/all_gather | solution.py:21
  109.0 5.8 %fusion.2 = f32[1024,704]{0,1:T(8,128)S(1)} fusion(bf16[2048,704]{0,1:T(8,128)(2,1)} %all-gather.7.cloned.1.call-done, bf16[1024,2048]{0,1:T(8,128)(2,1)} %fusion.1), kind=kOutput, calls=%fused_computation.10 | convolution fusion | flops 2952790016 | bytes 9961472 | tf_op jit(solution)/shard_map/dot_general | solution.py:24
  114.7 54.6 %all-gather.9.cloned.1.call-done = bf16[2048,704]{0,1:T(8,128)(2,1)} async-done(((bf16[256,704]{0,1:T(8,128)(2,1)}), bf16[2048,704]{0,1:T(8,128)(2,1)}) %all-gather.9.cloned.1.call-update) | async-done | bytes 2883600 | tf_op jit(solution)/shard_map/all_gather | solution.py:22
  169.4 7.5 %multiply_convert_fusion = bf16[1024,704]{0,1:T(8,128)(2,1)} fusion(f32[1024,704]{0,1:T(8,128)S(1)} %fusion.2, bf16[2048,704]{0,1:T(8,128)(2,1)} %all-gather.9.cloned.1.call-done, bf16[1024,2048]{0,1:T(8,128)(2,1)} %fusion.1), kind=kOutput, calls=%fused_computation.5 | convolution fusion | flops 2957115392 | bytes 11403264 | tf_op jit(solution)/shard_map/dot_general | solution.py:25
  176.9 0.0 all-gather.13.cloned.1.call-update
  176.9 50.6 %all-gather.11.cloned.1.call-done = bf16[2816,512]{1,0:T(8,128)(2,1)} async-done(((bf16[352,512]{1,0:T(8,128)(2,1)}), bf16[2816,512]{1,0:T(8,128)(2,1)}) %all-gather.11.cloned.1.call-update) | async-done | bytes 2883600 | tf_op jit(solution)/shard_map/all_gather | solution.py:27
  227.5 64.5 %all_to_all.19 = bf16[4,704,512]{2,1,0:T(8,128)(2,1)S(1)} all-to-all(bf16[4,704,512]{2,1,0:T(8,128)(2,1)} %bitcast.21), channel_id=1, replica_groups=mesh['fs'=8,'tp'=4] {'tp'}, dimensions={0} | all-to-all | bytes 5767168 | tf_op jit(solution)/shard_map/all_to_all | solution.py:28
  292.0 2.0 copy.16
  294.0 0.0 copy-start
  294.1 3.8 %all-gather.13.cloned.1.call-done = bf16[1024,2816]{0,1:T(8,128)(2,1)} async-done(((bf16[1024,704]{0,1:T(8,128)(2,1)}), bf16[1024,2816]{0,1:T(8,128)(2,1)}) %all-gather.13.cloned.1.call-update) | async-done | bytes 5767184 | tf_op jit(solution)/shard_map/all_gather | solution.py:30
  297.8 7.7 %convolution_convert_fusion = bf16[1024,512]{1,0:T(8,128)(2,1)} fusion(bf16[1024,2816]{0,1:T(8,128)(2,1)} %all-gather.13.cloned.1.call-done, bf16[2816,512]{1,0:T(8,128)(2,1)} %all-gather.11.cloned.1.call-done), kind=kOutput, calls=%fused_computation.6 | convolution fusion | flops 2953314304 | bytes 9699328 | tf_op jit(solution)/shard_map/dot_general | solution.py:29
  305.5 0.0 copy-done
  305.5 0.0 copy-start.1
  305.5 1.6 copy.19
  307.0 1.3 copy-done.1
  308.3 1.6 copy.20
  (1 shorter events, 0.0 us)
Async XLA Ops:
  7.2 3.9 %copy-start.2 = (f32[352,512]{1,0:T(8,128)S(1)}, f32[352,512]{1,0:T(8,128)}, u32[]{:S(2)}) copy-start(f32[352,512]{1,0:T(8,128)} %param.9) | copy-start | bytes 2162692
  7.2 39.6 %all-gather.15.cloned.1.call-start = ((), (), s32[]{:S(2)}) async-start(), calls=%async_computation.5 | async-start | bytes 5242880 | tf_op jit(solution)/shard_map/all_gather | solution.py:14
  7.9 101.1 %all-gather.7.cloned.1.call-start = ((), (), s32[]{:S(2)}) async-start(), calls=%async_computation.1 | async-start | bytes 3244032 | tf_op jit(solution)/shard_map/all_gather | solution.py:21
  10.3 159.1 %all-gather.9.cloned.1.call-start = ((), (), s32[]{:S(2)}) async-start(), calls=%async_computation.2 | async-start | bytes 3244032 | tf_op jit(solution)/shard_map/all_gather | solution.py:22
  11.0 216.5 %all-gather.11.cloned.1.call-start = ((), (), s32[]{:S(2)}) async-start(), calls=%async_computation.3 | async-start | bytes 3244032 | tf_op jit(solution)/shard_map/all_gather | solution.py:27
  11.9 285.9 %all-gather.13.cloned.1.call-start = ((), (), s32[]{:S(2)}) async-start(), calls=%async_computation.4 | async-start | bytes 7208960 | tf_op jit(solution)/shard_map/all_gather | solution.py:30
  294.0 11.4 %copy-start = (bf16[2048,704]{0,1:T(8,128)(2,1)S(1)}, bf16[2048,704]{0,1:T(8,128)(2,1)}, u32[]{:S(2)}) copy-start(bf16[2048,704]{0,1:T(8,128)(2,1)} %all-gather.7.cloned.1.call-done) | copy-start | bytes 8650756
  305.5 2.9 copy-start.1
Sparse Core Ops, SparseCore 0:
  9.5 37.1 all-gather.14
  49.4 59.5 all-gather.6
  111.6 57.7 all-gather.8
  172.0 55.4 all-gather.10
  229.5 68.2 all-gather.12
